TPU v7x, 32 devices: a whole 2x2x4 slice. The times are simulated.
32 devices in a mesh: dp: 4 (over y, x), kv: 4 (over z), tp: 2 (over core).
Axes of the slice: x: 2, y: 2, z: 4, core: 2. Of those that a mesh axis runs over, the one named last changes fastest.
Arguments:
- tokens: bfloat16 [16, 16, 2048], P('dp', None, 'kv'), may hold values from -6 to 6
- norm_gain: float32 [2048], P('kv'), may hold values from 0.1 to 1.9
- w_query: bfloat16 [2048, 1024], P('kv', 'tp'), may hold values from -0.125 to 0.125
- w_key: bfloat16 [2048, 1024], P('kv', 'tp'), may hold values from -0.125 to 0.125
- w_value: bfloat16 [2048, 1024], P('kv', 'tp'), may hold values from -0.125 to 0.125
- w_forget: bfloat16 [2048, 16], replicated, may hold values from -0.125 to 0.125
- forget_bias: float32 [16], replicated, may hold values from -2 to 4
- query_gain: float32 [64], replicated, may hold values from 0.1 to 1.9
- key_gain: float32 [64], replicated, may hold values from 0.1 to 1.9
- head_gain: float32 [64], replicated, may hold values from 0.1 to 1.9
- w_out: bfloat16 [1024, 2048], P('tp', 'kv'), may hold values from -0.1875 to 0.1875
- key_cache: bfloat16 [16, 2048, 1024], P('dp', 'kv', 'tp'), may hold values from -240 to 240
- value_cache: bfloat16 [16, 2048, 1024], P('dp', 'kv', 'tp'), may hold values from -6 to 6
- gate_cache: float32 [16, 16, 2048], P('dp', 'tp', 'kv'), may hold values from -242 to 0, as said below
- lengths: int32 [16], P('dp'), may hold values from 1005 to 2028
- accepted: int32 [16], P('dp'), may hold values from 0 to 4
- parents: int32 [16, 16], P('dp'), may hold values from -1 to 14, as said below
Outputs:
- layer_out: bfloat16 [16, 16, 2048], P('dp', None, 'kv')
- new_keys: bfloat16 [16, 2048, 1024], P('dp', 'kv', 'tp')
- new_values: bfloat16 [16, 2048, 1024], P('dp', 'kv', 'tp')
- proposal_gates: float32 [16, 16, 16], P('dp', None, 'tp')
Inputs may be any that keep to these rules, and one draw needn't show every extreme that they name: `gate_cache`: each entry is the running sum of log forget gates up to its position, so entries never rise along positions; entries at and after lengths hold the last step's proposals in order. `parents`: proposal 0 follows the last accepted token (parent -1); every other proposal's parent is one of the three proposals before it.
All inputs are finite; a program needn't handle non-finite values.
Results may differ from a plain program's by a relative error of at most 0.0051.
The roundings to bfloat16 on the way count: a program that leaves them out, or rounds other values in their place, can miss the bound.
Values may be sent and summed in bfloat16 or wider, within the bound.
A program may use at most 64 MiB of HBM per device.

v0:
```python
import jax
import jax.numpy as jnp
from jax import lax
from jax.sharding import PartitionSpec as P

EPSILON = 1e-06
MASKED = -1e30


def head_norm(head_rows, gain_vec):
    mean_square = jnp.mean(head_rows * head_rows, axis=-1, keepdims=True)
    return head_rows * lax.rsqrt(mean_square + EPSILON) * gain_vec


def ancestry(parents):
    count_all = parents.shape[1]
    step_ids = jnp.arange(count_all, dtype=jnp.int32)
    step_matrix = (parents[:, :, None] == step_ids[None, None, :]).astype(jnp.float32)
    identity = jnp.broadcast_to(jnp.eye(count_all, dtype=jnp.float32), step_matrix.shape)

    def extend(turn_index, ancestors):
        return identity + jnp.einsum(
            "sij,sjk->sik", step_matrix, ancestors, precision=lax.Precision.HIGHEST
        )

    return lax.fori_loop(0, count_all, extend, identity)


def combine(earlier, later):
    earlier_max, earlier_total, earlier_sum = earlier
    later_max, later_total, later_sum = later
    row_max = jnp.maximum(earlier_max, later_max)
    earlier_scale = jnp.exp(earlier_max - row_max)
    later_scale = jnp.exp(later_max - row_max)
    spread = earlier_max.shape + (-1,)
    joined = (
        earlier_sum.reshape(spread) * earlier_scale[..., None]
        + later_sum.reshape(spread) * later_scale[..., None]
    )
    return (
        row_max,
        earlier_total * earlier_scale + later_total * later_scale,
        joined.reshape(earlier_sum.shape),
    )


def block_part(scores, live_mask, block_values):
    seq_count, heads_local, prop_count, key_count = scores.shape
    row_max = jnp.max(scores, axis=3)
    weights = jnp.where(live_mask, jnp.exp(scores - row_max[..., None]), 0.0)
    row_total = jnp.sum(weights, axis=3)
    weighted = jnp.einsum(
        "shpk,skhd->sphd",
        weights.astype(jnp.bfloat16),
        block_values,
        preferred_element_type=jnp.float32,
    )
    return (
        jnp.transpose(row_max, (0, 2, 1)),
        jnp.transpose(row_total, (0, 2, 1)),
        weighted.reshape(seq_count, prop_count, -1),
    )


def finish_rows(row_sums, inverse, query_gain, key_gain, heads_local):
    head_width = row_sums.shape[1] // 3
    head_size = head_width // heads_local
    row_count = row_sums.shape[0]
    raw_sums = row_sums * inverse[:, None]
    queries = head_norm(
        raw_sums[:, :head_width].reshape(row_count, heads_local, head_size), query_gain
    )
    keyed = head_norm(
        raw_sums[:, head_width : 2 * head_width].reshape(row_count, heads_local, head_size),
        key_gain,
    )
    return jnp.concatenate(
        [
            queries.reshape(row_count, head_width),
            keyed.reshape(row_count, head_width),
            raw_sums[:, 2 * head_width :],
        ],
        axis=1,
    ).astype(jnp.bfloat16)


def flatten_part(part_triple, rows_all):
    part_max, part_total, part_sum = part_triple
    return (
        part_max.reshape(rows_all, -1),
        part_total.reshape(rows_all, -1),
        part_sum.reshape(rows_all, -1),
    )


def shards(
    tokens,
    norm_gain,
    w_query,
    w_key,
    w_value,
    w_forget,
    forget_bias,
    query_gain,
    key_gain,
    head_gain,
    w_out,
    key_cache,
    value_cache,
    gate_cache,
    lengths,
    accepted,
    parents,
):
    seq_count, prop_count, width_in = tokens.shape
    pos_dev = key_cache.shape[1]
    heads_local = gate_cache.shape[1]
    head_width = key_cache.shape[2]
    head_size = head_width // heads_local
    rows_all = seq_count * prop_count
    full_width = w_forget.shape[0]
    kv_index = lax.axis_index("kv")
    tp_index = lax.axis_index("tp")
    flattened = tokens.reshape(rows_all, width_in).astype(jnp.float32)
    squares = jnp.sum(flattened * flattened, axis=1)
    scaled = (flattened * norm_gain).astype(jnp.bfloat16)
    w_rows = lax.dynamic_slice_in_dim(w_forget, kv_index * width_in, width_in, 0)
    gate_part = jnp.dot(scaled, w_rows, preferred_element_type=jnp.float32)
    w_joined = jnp.concatenate([w_query, w_key, w_value], axis=1)
    summed, gate_sum, square_sum = lax.psum(
        (jnp.dot(scaled, w_joined, preferred_element_type=jnp.float32), gate_part, squares), "kv"
    )
    inverse = lax.rsqrt(square_sum / full_width + EPSILON)
    joined = finish_rows(summed, inverse, query_gain, key_gain, heads_local)
    log_all = jax.nn.log_sigmoid(gate_sum * inverse[:, None] + forget_bias)
    log_own = lax.dynamic_slice_in_dim(log_all, tp_index * heads_local, heads_local, 1)
    log_own = log_own.reshape(seq_count, prop_count, heads_local)
    queries = joined[:, :head_width].reshape(seq_count, prop_count, heads_local, head_size)
    keys_new = joined[:, head_width : 2 * head_width].reshape(
        seq_count, prop_count, heads_local, head_size
    )
    values_new = joined[:, 2 * head_width :].reshape(seq_count, prop_count, heads_local, head_size)
    ancestors = ancestry(parents)
    path_sum = jnp.einsum("sij,sjh->sih", ancestors, log_own, precision=lax.Precision.HIGHEST)
    base_pos = lengths + accepted
    positions = kv_index * pos_dev + jnp.arange(pos_dev, dtype=jnp.int32)
    score_scale = head_size ** (-0.5)
    cached_keys = key_cache.reshape(seq_count, pos_dev, heads_local, head_size)
    cached_values = value_cache.reshape(seq_count, pos_dev, heads_local, head_size)
    scores = jnp.einsum("sphd,skhd->shpk", queries, cached_keys, preferred_element_type=jnp.float32)
    scores = scores * score_scale - gate_cache[:, :, None, :]
    live_mask = (positions[None, :] < base_pos[:, None])[:, None, None, :]
    scores = jnp.where(live_mask, scores, MASKED)
    local_part = block_part(scores, live_mask, cached_values)
    hit_mask = positions[None, :] == (base_pos - 1)[:, None]
    boundary_local = jnp.sum(jnp.where(hit_mask[:, None, :], gate_cache, 0.0), axis=2)
    tree_live = (ancestors > 0.5)[:, None, :, :]
    boundary = lax.psum(boundary_local, "kv")
    flat_max, flat_total, flat_sum = flatten_part(local_part, rows_all)
    got_max, got_total, got_sum = (
        lax.all_to_all(flat_max[None], "kv", split_axis=1, concat_axis=0, tiled=True),
        lax.all_to_all(flat_total[None], "kv", split_axis=1, concat_axis=0, tiled=True),
        lax.all_to_all(flat_sum[None], "kv", split_axis=1, concat_axis=0, tiled=True),
    )
    top = jnp.max(got_max, axis=0)
    factors = jnp.exp(got_max - top[None])
    own_rows = got_max.shape[1]
    summed_rows = jnp.sum(
        got_sum.reshape(got_sum.shape[0], own_rows, heads_local, head_size) * factors[..., None],
        axis=0,
    )
    merged = (top, jnp.sum(got_total * factors, axis=0), summed_rows.reshape(own_rows, head_width))
    tree_scores = jnp.einsum(
        "sphd,sjhd->shpj", queries, keys_new, preferred_element_type=jnp.float32
    )
    tree_scores = (
        tree_scores * score_scale
        - jnp.transpose(path_sum, (0, 2, 1))[:, :, None, :]
        - boundary[:, :, None, None]
    )
    tree_scores = jnp.where(tree_live, tree_scores, MASKED)
    tree_max, tree_total, tree_sum = flatten_part(
        block_part(tree_scores, tree_live, values_new), rows_all
    )
    row_lower = kv_index * own_rows
    merged = combine(
        merged,
        (
            lax.dynamic_slice_in_dim(tree_max, row_lower, own_rows, 0),
            lax.dynamic_slice_in_dim(tree_total, row_lower, own_rows, 0),
            lax.dynamic_slice_in_dim(tree_sum, row_lower, own_rows, 0),
        ),
    )
    row_max, row_total, weighted = merged
    attended = weighted.reshape(own_rows, heads_local, head_size) / row_total[..., None]
    own_normed = head_norm(attended, head_gain).astype(jnp.bfloat16).reshape(own_rows, head_width)
    normed = lax.all_gather(own_normed, "kv", axis=0, tiled=True)
    out_term = jnp.dot(normed, w_out, preferred_element_type=jnp.float32)
    layer_out = lax.psum(out_term.astype(jnp.bfloat16), "tp")
    layer_out = layer_out.reshape(seq_count, prop_count, -1)
    new_rows = jnp.concatenate(
        [
            keys_new.reshape(seq_count, prop_count, head_width),
            values_new.reshape(seq_count, prop_count, head_width),
        ],
        axis=2,
    )
    slot_index = positions[None, :, None] - base_pos[:, None, None]
    placing = slot_index == jnp.arange(prop_count, dtype=jnp.int32)[None, None, :]
    written = jnp.einsum(
        "skp,spc->skc", placing.astype(jnp.bfloat16), new_rows, preferred_element_type=jnp.float32
    ).astype(jnp.bfloat16)
    hit_rows = jnp.any(placing, axis=2)[..., None]
    new_keys = jnp.where(hit_rows, written[..., :head_width], key_cache)
    new_values = jnp.where(hit_rows, written[..., head_width:], value_cache)
    return (layer_out, new_keys, new_values, log_own)


def solution(mesh):
    placed = (
        P("dp", None, "kv"),
        P("kv"),
        P("kv", "tp"),
        P("kv", "tp"),
        P("kv", "tp"),
        P(),
        P(),
        P(),
        P(),
        P(),
        P("tp", "kv"),
        P("dp", "kv", "tp"),
        P("dp", "kv", "tp"),
        P("dp", "tp", "kv"),
        P("dp"),
        P("dp"),
        P("dp", None),
    )
    return jax.shard_map(
        shards,
        mesh=mesh,
        in_specs=placed,
        out_specs=(
            P("dp", None, "kv"),
            P("dp", "kv", "tp"),
            P("dp", "kv", "tp"),
            P("dp", None, "tp"),
        ),
        check_vma=False,
    )
```

profile of v0, /device:TPU:0, one launch (start us, length us, event | category | flops | bytes accessed | tf_op | source)
XLA Modules:
  0.0 129.3 jit_solution(6320880123169172122)
XLA Ops:
  7.2 0.9 fusion.29
  8.3 2.6 %fusion.6 = f32[64,1536]{1,0:T(8,128)} fusion(bf16[64,512]{1,0:T(8,128)(2,1)S(1)} %fusion.29, bf16[512,512]{1,0:T(8,128)(2,1)} %param.23, bf16[512,512]{1,0:T(8,128)(2,1)} %param.22, bf16[512,512]{1,0:T(8,128)(2,1)} %param.21), kind=kOutput, calls=%fused_computation.9 | convolution fusion | flops 105381888 | bytes 2031616 | tf_op jit(solution)/shard_map/dot_general | solution.py:131
  11.2 4.2 %while.11 = (s32[]{:T(128)}, f32[4,16,16]{2,1,0:T(8,128)S(1)}, s32[4,16]{1,0:T(4,128)S(1)}, f32[16,16]{1,0:T(8,128)S(1)}, s32[]{:T(128)}) while((s32[]{:T(128)}, f32[4,16,16]{2,1,0:T(8,128)S(1)}, s32[4,16]{1,0:T(4,128)S(1)}, f32[16,16]{1,0:T(8,128)S(1)}, s32[]{:T(128)}) %tuple.50), condition=%wide.region_8.9_spmd.clone, body=%wide.region_7.8_spmd.clone.sunk | while | flops 199682 | bytes 17725 | solution.py:26
  11.3 0.2 convolution_add_fusion.2
  11.5 0.2 convolution_add_fusion.2
  11.8 0.2 convolution_add_fusion.2
  12.1 0.2 convolution_add_fusion.2
  12.3 0.2 convolution_add_fusion.2
  12.6 0.2 convolution_add_fusion.2
  12.8 0.2 convolution_add_fusion.2
  13.1 0.2 convolution_add_fusion.2
  13.4 0.2 convolution_add_fusion.2
  13.6 0.2 convolution_add_fusion.2
  13.9 0.2 convolution_add_fusion.2
  14.2 0.2 convolution_add_fusion.2
  14.4 0.2 convolution_add_fusion.2
  14.7 0.2 convolution_add_fusion.2
  15.0 0.2 convolution_add_fusion.2
  15.6 0.8 fusion.39
  16.4 20.4 %all-reduce = (f32[64]{0:T(128)S(1)}, f32[4,8]{1,0:T(4,128)S(1)}, f32[64,16]{0,1:T(8,128)S(1)}) all-reduce(f32[64]{0:T(128)S(1)} %reduce_sum.86, f32[4,8]{1,0:T(4,128)S(1)} %select_reduce_fusion, f32[64,16]{0,1:T(8,128)S(1)} %fusion.39), channel_id=1, replica_groups=mesh['dp'=4,'kv'=4,'tp'=2] {'kv'}, use_global_device_ids=true, to_apply=%region_2.0 | all-reduce | flops 1120 | bytes 8960 | tf_op jit(solution)/shard_map/psum | solution.py:130
  37.4 4.3 %copy.136 = bf16[4,512,512]{1,2,0:T(8,128)(2,1)} copy(bf16[4,512,512]{2,1,0:T(8,128)(2,1)} %param.30) | data formatting | bytes 4194304 | tf_op args[11]
  41.7 2.4 %copy.138 = bf16[4,512,512]{1,2,0:T(8,128)(2,1)} copy(bf16[4,512,512]{2,1,0:T(8,128)(2,1)S(1)} %copy-done.1) | data formatting | bytes 4194304 | tf_op args[12]
  44.3 6.7 %all-reduce.4.cloned.1.call-done = f32[64,1536]{1,0:T(8,128)} async-done(((f32[64,1536]{1,0:T(8,128)}), f32[64,1536]{1,0:T(8,128)}) %all-reduce.4.cloned.1.call-update) | async-done | bytes 393232 | tf_op jit(solution)/shard_map/psum | solution.py:130
  51.0 1.1 broadcast_multiply_fusion
  53.9 2.1 %fusion.57 = (f32[4,8,16]{2,1,0:T(8,128)S(1)}, f32[4,8,16,512]{3,2,1,0:T(8,128)S(1)}) fusion(f32[4,8,512]{2,1,0:T(8,128)S(1)} %copy-done.3, bf16[4,512,8,64]{1,3,2,0:T(8,128)(2,1)} %bitcast.48, bf16[4,16,8,64]{3,2,1,0:T(8,128)(2,1)S(1)} %reshape.230, pred[4,512]{1,0:T(4,128)(4,1)S(1)} %get-tuple-element.90), kind=kOutput, calls=%fused_computation.96 | convolution fusion | flops 34602496 | bytes 3280896 | tf_op jit(solution)/shard_map/sphd,skhd->shpk/dot_general | solution.py:150
  56.0 0.3 fusion.17
  56.4 0.5 broadcast.155
  57.0 0.7 reduce.2
  57.7 0.7 reshape.243
  58.3 3.4 %all-to-all-start.2 = ((f32[4,1,128]{2,1,0:T(1,128)}), f32[4,1,128]{2,1,0:T(1,128)S(1)}, u32[]{:S(2)}, u32[]{:S(2)}) async-start(f32[4,1,128]{2,1,0:T(1,128)} %reshape.243), calls=%async_computation.2 | async-start | bytes 4096 | tf_op jit(solution)/shard_map/all_to_all | solution.py:162
  61.8 2.3 %convolution_bitcast_fusion = f32[4,16,8,64]{3,1,2,0:T(8,128)S(1)} fusion(bf16[4,512,8,64]{1,3,2,0:T(8,128)(2,1)} %bitcast.47, f32[4,8,16,512]{3,2,1,0:T(8,128)S(1)} %get-tuple-element.95, f32[4,8,16]{2,1,0:T(8,128)S(1)} %get-tuple-element.94, pred[4,512]{1,0:T(4,128)(4,1)S(1)} %get-tuple-element.90), kind=kOutput, calls=%fused_computation.21 | convolution fusion | flops 34340864 | bytes 3280896 | tf_op jit(solution)/shard_map/shpk,skhd->sphd/dot_general | solution.py:52
  64.1 3.2 %convolution_convert_fusion = bf16[4,512,1024]{2,1,0:T(8,128)(2,1)} fusion(bf16[4,16,512]{2,1,0:T(8,128)(2,1)S(1)} %bitcast.50, bf16[4,16,512]{2,1,0:T(8,128)(2,1)S(1)} %bitcast.49, s32[4,512]{1,0:T(4,128)S(1)} %broadcast_subtract_fusion), kind=kOutput, calls=%fused_computation.6 | convolution fusion | flops 69500928 | bytes 4333568 | tf_op jit(solution)/shard_map/skp,spc->skc/dot_general | solution.py:210
  67.3 0.2 fusion.56
  67.6 0.2 convolution_bitcast_fusion.1
  68.2 0.7 reduce.4
  68.9 0.7 reshape.241
  69.6 5.1 %all-to-all-start.1 = ((f32[4,1,128]{2,1,0:T(1,128)}), f32[4,1,128]{2,1,0:T(1,128)S(1)}, u32[]{:S(2)}, u32[]{:S(2)}) async-start(f32[4,1,128]{2,1,0:T(1,128)} %reshape.241), calls=%async_computation.1 | async-start | bytes 4096 | tf_op jit(solution)/shard_map/all_to_all | solution.py:161
  75.0 0.8 broadcast_in_dim_reshape_reshape.4
  75.8 0.6 reduce.3
  76.6 3.6 %all-to-all-done.1 = f32[4,1,128]{2,1,0:T(1,128)S(1)} async-done(((f32[4,1,128]{2,1,0:T(1,128)}), f32[4,1,128]{2,1,0:T(1,128)S(1)}, u32[]{:S(2)}, u32[]{:S(2)}) %all-to-all-start.1) | async-done | bytes 2080 | tf_op jit(solution)/shard_map/all_to_all | solution.py:161
  80.1 3.3 %all-to-all-start = ((f32[1,64,512]{2,0,1:T(1,128)}), f32[1,64,512]{2,0,1:T(1,128)S(1)}, u32[]{:S(2)}, u32[]{:S(2)}) async-start(f32[1,64,512]{2,0,1:T(1,128)} %broadcast_in_dim_reshape_reshape.4), calls=%async_computation | async-start | bytes 262144 | tf_op jit(solution)/shard_map/all_to_all | solution.py:163
  83.5 0.6 reduce.5
  85.2 4.2 %all-to-all-done = f32[1,64,512]{2,0,1:T(1,128)S(1)} async-done(((f32[1,64,512]{2,0,1:T(1,128)}), f32[1,64,512]{2,0,1:T(1,128)S(1)}, u32[]{:S(2)}, u32[]{:S(2)}) %all-to-all-start) | async-done | bytes 131104 | tf_op jit(solution)/shard_map/all_to_all | solution.py:163
  90.1 13.1 %all_gather.3 = bf16[64,512]{1,0:T(8,128)(2,1)S(1)} all-gather(bf16[16,512]{1,0:T(8,128)(2,1)S(1)} %multiply_convert_fusion.2), channel_id=1, replica_groups=mesh['dp'=4,'kv'=4,'tp'=2] {'kv'}, dimensions={0}, use_global_device_ids=true | all-gather | bytes 81920 | tf_op jit(solution)/shard_map/all_gather | solution.py:197
  103.2 0.8 convolution_convert_fusion.1
  104.1 4.4 %slice_select_fusion = (bf16[4,512,512]{2,1,0:T(8,128)(2,1)}, bf16[4,512,512]{2,1,0:T(8,128)(2,1)}) fusion(bf16[4,512,512]{2,1,0:T(8,128)(2,1)S(1)} %copy-done.2, bf16[4,512,1024]{2,1,0:T(8,128)(2,1)} %convolution_convert_fusion, pred[4,512]{1,0:T(4,128)(4,1)S(1)} %fusion.32, bf16[4,512,512]{2,1,0:T(8,128)(2,1)} %param.30), kind=kLoop, calls=%fused_computation.7 | loop fusion | flops 2097152 | bytes 12584960 | tf_op jit(solution)/shard_map/jit(_where)/select_n | solution.py:215
  108.5 12.4 %all-reduce.6.cloned.1.call-done = bf16[4,16,512]{2,1,0:T(8,128)(2,1)} async-done(((bf16[4,16,512]{2,1,0:T(8,128)(2,1)}), bf16[4,16,512]{2,1,0:T(8,128)(2,1)}) %all-reduce.6.cloned.1.call-update) | async-done | bytes 65552 | tf_op jit(solution)/shard_map/psum | solution.py:199
  121.0 1.5 %copy.192 = bf16[4,16,512]{2,1,0:T(8,128)(2,1)} copy(bf16[4,16,512]{2,1,0:T(8,128)(2,1)} %all-reduce.6.cloned.1.call-done) | data formatting | bytes 131072
  (122 shorter events, 5.9 us)
Async XLA Ops:
  7.2 96.0 %copy-start = (bf16[512,512]{1,0:T(8,128)(2,1)S(1)}, bf16[512,512]{1,0:T(8,128)(2,1)}, u32[]{:S(2)}) copy-start(bf16[512,512]{1,0:T(8,128)(2,1)} %param.29) | copy-start | bytes 1572868
  7.2 43.8 %all-reduce.4.cloned.1.call-start = ((), (), s32[]{:S(2)}) async-start(), calls=%async_computation.3 | async-start | bytes 786432 | tf_op jit(solution)/shard_map/psum | solution.py:130
  8.1 2.7 %copy-start.4 = (bf16[4,16,512]{2,1,0:T(8,128)(2,1)S(1)}, bf16[4,16,512]{2,1,0:T(8,128)(2,1)}, u32[]{:S(2)}) copy-start(bf16[4,16,512]{2,1,0:T(8,128)(2,1)} %param.19) | copy-start | bytes 196612
  8.2 2.9 %copy-start.11 = (s32[4]{0:T(128)S(1)}, s32[4]{0:T(128)}, u32[]{:S(2)}) copy-start(s32[4]{0:T(128)} %param.33) | copy-start | bytes 52
  8.2 2.9 %copy-start.12 = (s32[4]{0:T(128)S(1)}, s32[4]{0:T(128)}, u32[]{:S(2)}) copy-start(s32[4]{0:T(128)} %param.34) | copy-start | bytes 52
  8.2 3.0 %copy-start.6 = (s32[4,16]{1,0:T(4,128)S(1)}, s32[4,16]{1,0:T(4,128)}, u32[]{:S(2)}) copy-start(s32[4,16]{1,0:T(4,128)} %param.35) | copy-start | bytes 772
  8.2 7.3 %copy-start.3 = (f32[4,8,512]{2,1,0:T(8,128)S(1)}, f32[4,8,512]{2,1,0:T(8,128)}, u32[]{:S(2)}) copy-start(f32[4,8,512]{2,1,0:T(8,128)} %param.32) | copy-start | bytes 196612
  8.2 28.7 %copy-start.7 = (f32[16]{0:T(128)S(1)}, f32[16]{0:T(128)}, u32[]{:S(2)}) copy-start(f32[16]{0:T(128)} %param.25) | copy-start | bytes 196
  8.2 28.8 %copy-start.8 = (f32[64]{0:T(128)S(1)}, f32[64]{0:T(128)}, u32[]{:S(2)}) copy-start(f32[64]{0:T(128)} %param.26) | copy-start | bytes 772
  8.2 28.8 %copy-start.9 = (f32[64]{0:T(128)S(1)}, f32[64]{0:T(128)}, u32[]{:S(2)}) copy-start(f32[64]{0:T(128)} %param.27) | copy-start | bytes 772
  8.2 28.9 %copy-start.10 = (f32[64]{0:T(128)S(1)}, f32[64]{0:T(128)}, u32[]{:S(2)}) copy-start(f32[64]{0:T(128)} %param.28) | copy-start | bytes 772
  37.4 6.7 %copy-start.5 = (f32[4,16,8]{1,2,0:T(8,128)}, f32[4,16,8]{1,2,0:T(8,128)S(1)}, u32[]{:S(2)}) copy-start(f32[4,16,8]{1,2,0:T(8,128)S(1)} %copy.148) | copy-start | bytes 6148
  37.4 4.3 %copy-start.1 = (bf16[4,512,512]{2,1,0:T(8,128)(2,1)S(1)}, bf16[4,512,512]{2,1,0:T(8,128)(2,1)}, u32[]{:S(2)}) copy-start(bf16[4,512,512]{2,1,0:T(8,128)(2,1)} %param.31) | copy-start | bytes 6291460
  58.3 11.2 %all-to-all-start.2 = ((f32[4,1,128]{2,1,0:T(1,128)}), f32[4,1,128]{2,1,0:T(1,128)S(1)}, u32[]{:S(2)}, u32[]{:S(2)}) async-start(f32[4,1,128]{2,1,0:T(1,128)} %reshape.243), calls=%async_computation.2 | async-start | bytes 4096 | tf_op jit(solution)/shard_map/all_to_all | solution.py:162
  69.6 10.6 %all-to-all-start.1 = ((f32[4,1,128]{2,1,0:T(1,128)}), f32[4,1,128]{2,1,0:T(1,128)S(1)}, u32[]{:S(2)}, u32[]{:S(2)}) async-start(f32[4,1,128]{2,1,0:T(1,128)} %reshape.241), calls=%async_computation.1 | async-start | bytes 4096 | tf_op jit(solution)/shard_map/all_to_all | solution.py:161
  75.0 29.1 %copy-start.2 = (bf16[4,512,512]{2,1,0:T(8,128)(2,1)S(1)}, bf16[4,512,512]{2,1,0:T(8,128)(2,1)}, u32[]{:S(2)}) copy-start(bf16[4,512,512]{2,1,0:T(8,128)(2,1)} %param.31) | copy-start | bytes 6291460
  80.1 9.2 %all-to-all-start = ((f32[1,64,512]{2,0,1:T(1,128)}), f32[1,64,512]{2,0,1:T(1,128)S(1)}, u32[]{:S(2)}, u32[]{:S(2)}) async-start(f32[1,64,512]{2,0,1:T(1,128)} %broadcast_in_dim_reshape_reshape.4), calls=%async_computation | async-start | bytes 262144 | tf_op jit(solution)/shard_map/all_to_all | solution.py:163
  83.5 37.5 %all-reduce.6.cloned.1.call-start = ((), (), s32[]{:S(2)}) async-start(), calls=%async_computation.4 | async-start | bytes 131072 | tf_op jit(solution)/shard_map/psum | solution.py:199
Sparse Core Ops, SparseCore 0:
  11.0 39.9 all-reduce.3
  104.2 16.7 all-reduce.5
where the time goes:
time: 130 us; the launch traced here: 129 us
  blocking collectives  33.6 us (26%)
  waiting for transfers between devices  27 us (21%)
  matrix products  16.2 us (12%)
  local copies, waits for them, and re-layouts  14.8 us (11%)
  between operations  14.5 us (11%)
  starting transfers between devices  11.9 us (9%)
  other arithmetic  10.9 us (8%)
    psum x1, blocking collectives, shards(): lax.psum((jnp.dot(scaled, w_joined, preferred_element_type=jnp.float32),...  20.4 us
    all_gather x1, blocking collectives, shards(): normed = lax.all_gather(own_normed, 'kv', axis=0, tiled=True)  13.1 us
    psum x1, waiting for transfers between devices, shards(): layer_out = lax.psum(out_term.astype(jnp.bfloat16), 'tp')  12.4 us
    unnamed x34, local copies, waits for them, and re-layouts  10.3 us
    psum x1, waiting for transfers between devices, shards(): lax.psum((jnp.dot(scaled, w_joined, preferred_element_type=jnp.float32),...  6.72 us
    all_to_all x1, starting transfers between devices, shards(): lax.all_to_all(flat_max[None], 'kv', split_axis=1, concat_axis=0, tiled=T...  5.09 us
    select_n x1, other arithmetic, shards(): new_values = jnp.where(hit_rows, written[..., head_width:], value_cache)  4.45 us
    all_to_all x1, waiting for transfers between devices, shards(): lax.all_to_all(flat_sum[None], 'kv', split_axis=1, concat_axis=0, tiled=T...  4.2 us
  transfers between devices with their start and end apart: 5, of which 4 were waited for; matrix products, arithmetic and copies ran while one was open for 22% of the time, Pallas kernels for 0%

commit v1 on v0

--- a/solution.py
+++ b/solution.py
@@ -157,8 +157,20 @@
     tree_live = (ancestors > 0.5)[:, None, :, :]
     boundary = lax.psum(boundary_local, "kv")
     flat_max, flat_total, flat_sum = flatten_part(local_part, rows_all)
+
+    def rows_put(z_in):
+        return jnp.concatenate(
+            lax.all_to_all(
+                jnp.stack(jnp.split(z_in, lax.psum(1, axis_name="kv"), axis=1), axis=0),
+                "kv",
+                split_axis=0,
+                concat_axis=0,
+            ),
+            axis=0,
+        )
+
     got_max, got_total, got_sum = (
-        lax.all_to_all(flat_max[None], "kv", split_axis=1, concat_axis=0, tiled=True),
+        rows_put(flat_max[None]),
         lax.all_to_all(flat_total[None], "kv", split_axis=1, concat_axis=0, tiled=True),
         lax.all_to_all(flat_sum[None], "kv", split_axis=1, concat_axis=0, tiled=True),
     )

time: 130 us -> 131 us (level)
    all_to_all x1, waiting for transfers between devices: 0.01 us -> 4.77 us  [shards(): lax.all_to_all(flat_total[None], 'kv', split_axis=1, concat_axis=0, tiled...]
    all_to_all x1, waiting for transfers between devices: 3.58 us -> 0.01 us  [rows_put(): lax.all_to_all(jnp.stack(jnp.split(z_in, lax.psum(1, axis_name='kv'), axi...]
    all_to_all x1, starting transfers between devices: 3.44 us -> 5.09 us  [shards(): lax.all_to_all(flat_total[None], 'kv', split_axis=1, concat_axis=0, tiled...]
    all_to_all x1, starting transfers between devices: 5.09 us -> 3.43 us  [rows_put(): lax.all_to_all(jnp.stack(jnp.split(z_in, lax.psum(1, axis_name='kv'), axi...]
where the time goes in v1:
time: 131 us; the launch traced here: 130 us
  blocking collectives  33.6 us (26%)
  waiting for transfers between devices  27.8 us (21%)
  matrix products  16.2 us (12%)
  local copies, waits for them, and re-layouts  15.2 us (12%)
  between operations  14.5 us (11%)
  starting transfers between devices  11.9 us (9%)
  other arithmetic  10.2 us (8%)
    psum x1, blocking collectives, shards(): lax.psum((jnp.dot(scaled, w_joined, preferred_element_type=jnp.float32),...  20.4 us
    all_gather x1, blocking collectives, shards(): normed = lax.all_gather(own_normed, 'kv', axis=0, tiled=True)  13.1 us
    psum x1, waiting for transfers between devices, shards(): layer_out = lax.psum(out_term.astype(jnp.bfloat16), 'tp')  12.4 us
    unnamed x34, local copies, waits for them, and re-layouts  10.3 us
    psum x1, waiting for transfers between devices, shards(): lax.psum((jnp.dot(scaled, w_joined, preferred_element_type=jnp.float32),...  6.72 us
    all_to_all x1, starting transfers between devices, shards(): lax.all_to_all(flat_total[None], 'kv', split_axis=1, concat_axis=0, tiled...  5.09 us
    all_to_all x1, waiting for transfers between devices, shards(): lax.all_to_all(flat_total[None], 'kv', split_axis=1, concat_axis=0, tiled...  4.77 us
    select_n x1, other arithmetic, shards(): new_values = jnp.where(hit_rows, written[..., head_width:], value_cache)  4.45 us
  transfers between devices with their start and end apart: 5, of which 4 were waited for; matrix products, arithmetic and copies ran while one was open for 22% of the time, Pallas kernels for 0%

profile of v1, /device:TPU:0, one launch (start us, length us, event | category | flops | bytes accessed | tf_op | source)
XLA Modules:
  0.0 129.8 jit_solution(11201349422121988197)
XLA Ops:
  7.2 0.9 fusion.29
  8.3 2.6 %fusion.6 = f32[64,1536]{1,0:T(8,128)} fusion(bf16[64,512]{1,0:T(8,128)(2,1)S(1)} %fusion.29, bf16[512,512]{1,0:T(8,128)(2,1)} %param.23, bf16[512,512]{1,0:T(8,128)(2,1)} %param.22, bf16[512,512]{1,0:T(8,128)(2,1)} %param.21), kind=kOutput, calls=%fused_computation.9 | convolution fusion | flops 105381888 | bytes 2031616 | tf_op jit(solution)/shard_map/dot_general | solution.py:131
  11.2 4.2 %while.11 = (s32[]{:T(128)}, f32[4,16,16]{2,1,0:T(8,128)S(1)}, s32[4,16]{1,0:T(4,128)S(1)}, f32[16,16]{1,0:T(8,128)S(1)}, s32[]{:T(128)}) while((s32[]{:T(128)}, f32[4,16,16]{2,1,0:T(8,128)S(1)}, s32[4,16]{1,0:T(4,128)S(1)}, f32[16,16]{1,0:T(8,128)S(1)}, s32[]{:T(128)}) %tuple.52), condition=%wide.region_8.9_spmd.clone, body=%wide.region_7.8_spmd.clone.sunk | while | flops 199682 | bytes 17725 | solution.py:26
  11.3 0.2 convolution_add_fusion.2
  11.5 0.2 convolution_add_fusion.2
  11.8 0.2 convolution_add_fusion.2
  12.1 0.2 convolution_add_fusion.2
  12.3 0.2 convolution_add_fusion.2
  12.6 0.2 convolution_add_fusion.2
  12.8 0.2 convolution_add_fusion.2
  13.1 0.2 convolution_add_fusion.2
  13.4 0.2 convolution_add_fusion.2
  13.6 0.2 convolution_add_fusion.2
  13.9 0.2 convolution_add_fusion.2
  14.2 0.2 convolution_add_fusion.2
  14.4 0.2 convolution_add_fusion.2
  14.7 0.2 convolution_add_fusion.2
  15.0 0.2 convolution_add_fusion.2
  15.2 0.2 convolution_add_fusion.2
  15.6 0.8 fusion.40
  16.4 20.4 %all-reduce = (f32[64]{0:T(128)S(1)}, f32[4,8]{1,0:T(4,128)S(1)}, f32[64,16]{0,1:T(8,128)S(1)}) all-reduce(f32[64]{0:T(128)S(1)} %reduce_sum.86, f32[4,8]{1,0:T(4,128)S(1)} %select_reduce_fusion, f32[64,16]{0,1:T(8,128)S(1)} %fusion.40), channel_id=1, replica_groups=mesh['dp'=4,'kv'=4,'tp'=2] {'kv'}, use_global_device_ids=true, to_apply=%region_2.0 | all-reduce | flops 1120 | bytes 8960 | tf_op jit(solution)/shard_map/psum | solution.py:130
  37.4 4.3 %copy.128 = bf16[4,512,512]{1,2,0:T(8,128)(2,1)} copy(bf16[4,512,512]{2,1,0:T(8,128)(2,1)} %param.30) | data formatting | bytes 4194304 | tf_op args[11]
  41.7 2.4 %copy.130 = bf16[4,512,512]{1,2,0:T(8,128)(2,1)} copy(bf16[4,512,512]{2,1,0:T(8,128)(2,1)S(1)} %copy-done.1) | data formatting | bytes 4194304 | tf_op args[12]
  44.3 6.7 %all-reduce.4.cloned.1.call-done = f32[64,1536]{1,0:T(8,128)} async-done(((f32[64,1536]{1,0:T(8,128)}), f32[64,1536]{1,0:T(8,128)}) %all-reduce.4.cloned.1.call-update) | async-done | bytes 393232 | tf_op jit(solution)/shard_map/psum | solution.py:130
  51.0 1.1 broadcast_multiply_fusion
  53.9 0.2 fusion.58
  54.3 0.2 convolution_bitcast_fusion.1
  54.7 2.1 %fusion.59 = (f32[4,8,16]{2,1,0:T(8,128)S(1)}, f32[4,8,16,512]{3,2,1,0:T(8,128)S(1)}) fusion(f32[4,8,512]{2,1,0:T(8,128)S(1)} %copy-done.3, bf16[4,512,8,64]{1,3,2,0:T(8,128)(2,1)} %bitcast.66, bf16[4,16,8,64]{3,2,1,0:T(8,128)(2,1)S(1)} %reshape.233, pred[4,512]{1,0:T(4,128)(4,1)S(1)} %get-tuple-element.90), kind=kOutput, calls=%fused_computation.102 | convolution fusion | flops 34602496 | bytes 3280896 | tf_op jit(solution)/shard_map/sphd,skhd->shpk/dot_general | solution.py:150
  57.0 0.7 reshape.245
  57.7 3.4 %all-to-all-start.1 = ((f32[4,1,128]{2,1,0:T(1,128)}), f32[4,1,128]{2,1,0:T(1,128)S(1)}, u32[]{:S(2)}, u32[]{:S(2)}) async-start(f32[4,1,128]{2,1,0:T(1,128)} %reshape.245), calls=%async_computation.1 | async-start | bytes 4096 | tf_op jit(solution)/shard_map/all_to_all | solution.py:163
  61.1 0.3 fusion.17
  61.4 2.3 %convolution_bitcast_fusion = f32[4,16,8,64]{3,1,2,0:T(8,128)S(1)} fusion(bf16[4,512,8,64]{1,3,2,0:T(8,128)(2,1)} %bitcast.65, f32[4,8,16,512]{3,2,1,0:T(8,128)S(1)} %get-tuple-element.95, f32[4,8,16]{2,1,0:T(8,128)S(1)} %get-tuple-element.94, pred[4,512]{1,0:T(4,128)(4,1)S(1)} %get-tuple-element.90), kind=kOutput, calls=%fused_computation.21 | convolution fusion | flops 34340864 | bytes 3280896 | tf_op jit(solution)/shard_map/shpk,skhd->sphd/dot_general | solution.py:52
  63.7 3.2 %convolution_convert_fusion = bf16[4,512,1024]{2,1,0:T(8,128)(2,1)} fusion(bf16[4,16,512]{2,1,0:T(8,128)(2,1)S(1)} %bitcast.68, bf16[4,16,512]{2,1,0:T(8,128)(2,1)S(1)} %bitcast.67, s32[4,512]{1,0:T(4,128)S(1)} %broadcast_subtract_fusion), kind=kOutput, calls=%fused_computation.6 | convolution fusion | flops 69500928 | bytes 4333568 | tf_op jit(solution)/shard_map/skp,spc->skc/dot_general | solution.py:222
  67.3 0.5 broadcast.155
  67.8 0.7 reduce.3
  68.5 0.7 reshape.247
  69.3 0.8 broadcast_in_dim_reshape_reshape.4
  70.1 5.1 %all-to-all-start.2 = ((f32[4,1,128]{2,1,0:T(1,128)}), f32[4,1,128]{2,1,0:T(1,128)S(1)}, u32[]{:S(2)}, u32[]{:S(2)}) async-start(f32[4,1,128]{2,1,0:T(1,128)} %reshape.247), calls=%async_computation.2 | async-start | bytes 4096 | tf_op jit(solution)/shard_map/all_to_all | solution.py:174
  75.2 0.6 reduce.5
  76.0 4.8 %all-to-all-done.2 = f32[4,1,128]{2,1,0:T(1,128)S(1)} async-done(((f32[4,1,128]{2,1,0:T(1,128)}), f32[4,1,128]{2,1,0:T(1,128)S(1)}, u32[]{:S(2)}, u32[]{:S(2)}) %all-to-all-start.2) | async-done | bytes 2080 | tf_op jit(solution)/shard_map/all_to_all | solution.py:174
  80.7 3.3 %all-to-all-start = ((f32[1,64,512]{2,0,1:T(1,128)}), f32[1,64,512]{2,0,1:T(1,128)S(1)}, u32[]{:S(2)}, u32[]{:S(2)}) async-start(f32[1,64,512]{2,0,1:T(1,128)} %broadcast_in_dim_reshape_reshape.4), calls=%async_computation | async-start | bytes 262144 | tf_op jit(solution)/shard_map/all_to_all | solution.py:175
  84.1 0.6 reduce.4
  86.2 3.8 %all-to-all-done = f32[1,64,512]{2,0,1:T(1,128)S(1)} async-done(((f32[1,64,512]{2,0,1:T(1,128)}), f32[1,64,512]{2,0,1:T(1,128)S(1)}, u32[]{:S(2)}, u32[]{:S(2)}) %all-to-all-start) | async-done | bytes 131104 | tf_op jit(solution)/shard_map/all_to_all | solution.py:175
  90.6 13.1 %all_gather.3 = bf16[64,512]{1,0:T(8,128)(2,1)S(1)} all-gather(bf16[16,512]{1,0:T(8,128)(2,1)S(1)} %multiply_convert_fusion.2), channel_id=1, replica_groups=mesh['dp'=4,'kv'=4,'tp'=2] {'kv'}, dimensions={0}, use_global_device_ids=true | all-gather | bytes 81920 | tf_op jit(solution)/shard_map/all_gather | solution.py:209
  103.8 0.8 convolution_convert_fusion.1
  104.6 4.4 %slice_select_fusion = (bf16[4,512,512]{2,1,0:T(8,128)(2,1)}, bf16[4,512,512]{2,1,0:T(8,128)(2,1)}) fusion(bf16[4,512,512]{2,1,0:T(8,128)(2,1)S(1)} %copy-done.2, bf16[4,512,1024]{2,1,0:T(8,128)(2,1)} %convolution_convert_fusion, pred[4,512]{1,0:T(4,128)(4,1)S(1)} %fusion.32, bf16[4,512,512]{2,1,0:T(8,128)(2,1)} %param.30), kind=kLoop, calls=%fused_computation.7 | loop fusion | flops 2097152 | bytes 12584960 | tf_op jit(solution)/shard_map/jit(_where)/select_n | solution.py:227
  109.1 12.4 %all-reduce.6.cloned.1.call-done = bf16[4,16,512]{2,1,0:T(8,128)(2,1)} async-done(((bf16[4,16,512]{2,1,0:T(8,128)(2,1)}), bf16[4,16,512]{2,1,0:T(8,128)(2,1)}) %all-reduce.6.cloned.1.call-update) | async-done | bytes 65552 | tf_op jit(solution)/shard_map/psum | solution.py:211
  121.5 1.5 %copy.183 = bf16[4,16,512]{2,1,0:T(8,128)(2,1)} copy(bf16[4,16,512]{2,1,0:T(8,128)(2,1)} %all-reduce.6.cloned.1.call-done) | data formatting | bytes 131072
  (131 shorter events, 6.2 us)
Async XLA Ops:
  7.2 96.6 %copy-start = (bf16[512,512]{1,0:T(8,128)(2,1)S(1)}, bf16[512,512]{1,0:T(8,128)(2,1)}, u32[]{:S(2)}) copy-start(bf16[512,512]{1,0:T(8,128)(2,1)} %param.29) | copy-start | bytes 1572868
  7.2 43.8 %all-reduce.4.cloned.1.call-start = ((), (), s32[]{:S(2)}) async-start(), calls=%async_computation.3 | async-start | bytes 786432 | tf_op jit(solution)/shard_map/psum | solution.py:130
  8.1 2.7 %copy-start.4 = (bf16[4,16,512]{2,1,0:T(8,128)(2,1)S(1)}, bf16[4,16,512]{2,1,0:T(8,128)(2,1)}, u32[]{:S(2)}) copy-start(bf16[4,16,512]{2,1,0:T(8,128)(2,1)} %param.19) | copy-start | bytes 196612
  8.2 2.9 %copy-start.11 = (s32[4]{0:T(128)S(1)}, s32[4]{0:T(128)}, u32[]{:S(2)}) copy-start(s32[4]{0:T(128)} %param.33) | copy-start | bytes 52
  8.2 2.9 %copy-start.12 = (s32[4]{0:T(128)S(1)}, s32[4]{0:T(128)}, u32[]{:S(2)}) copy-start(s32[4]{0:T(128)} %param.34) | copy-start | bytes 52
  8.2 3.0 %copy-start.6 = (s32[4,16]{1,0:T(4,128)S(1)}, s32[4,16]{1,0:T(4,128)}, u32[]{:S(2)}) copy-start(s32[4,16]{1,0:T(4,128)} %param.35) | copy-start | bytes 772
  8.2 7.3 %copy-start.3 = (f32[4,8,512]{2,1,0:T(8,128)S(1)}, f32[4,8,512]{2,1,0:T(8,128)}, u32[]{:S(2)}) copy-start(f32[4,8,512]{2,1,0:T(8,128)} %param.32) | copy-start | bytes 196612
  8.2 28.7 %copy-start.7 = (f32[16]{0:T(128)S(1)}, f32[16]{0:T(128)}, u32[]{:S(2)}) copy-start(f32[16]{0:T(128)} %param.25) | copy-start | bytes 196
  8.2 28.8 %copy-start.8 = (f32[64]{0:T(128)S(1)}, f32[64]{0:T(128)}, u32[]{:S(2)}) copy-start(f32[64]{0:T(128)} %param.26) | copy-start | bytes 772
  8.2 28.8 %copy-start.9 = (f32[64]{0:T(128)S(1)}, f32[64]{0:T(128)}, u32[]{:S(2)}) copy-start(f32[64]{0:T(128)} %param.27) | copy-start | bytes 772
  8.2 28.9 %copy-start.10 = (f32[64]{0:T(128)S(1)}, f32[64]{0:T(128)}, u32[]{:S(2)}) copy-start(f32[64]{0:T(128)} %param.28) | copy-start | bytes 772
  37.4 6.7 %copy-start.5 = (f32[4,16,8]{1,2,0:T(8,128)}, f32[4,16,8]{1,2,0:T(8,128)S(1)}, u32[]{:S(2)}) copy-start(f32[4,16,8]{1,2,0:T(8,128)S(1)} %copy.140) | copy-start | bytes 6148
  37.4 4.3 %copy-start.1 = (bf16[4,512,512]{2,1,0:T(8,128)(2,1)S(1)}, bf16[4,512,512]{2,1,0:T(8,128)(2,1)}, u32[]{:S(2)}) copy-start(bf16[4,512,512]{2,1,0:T(8,128)(2,1)} %param.31) | copy-start | bytes 6291460
  57.7 12.5 %all-to-all-start.1 = ((f32[4,1,128]{2,1,0:T(1,128)}), f32[4,1,128]{2,1,0:T(1,128)S(1)}, u32[]{:S(2)}, u32[]{:S(2)}) async-start(f32[4,1,128]{2,1,0:T(1,128)} %reshape.245), calls=%async_computation.1 | async-start | bytes 4096 | tf_op jit(solution)/shard_map/all_to_all | solution.py:163
  69.3 35.3 %copy-start.2 = (bf16[4,512,512]{2,1,0:T(8,128)(2,1)S(1)}, bf16[4,512,512]{2,1,0:T(8,128)(2,1)}, u32[]{:S(2)}) copy-start(bf16[4,512,512]{2,1,0:T(8,128)(2,1)} %param.31) | copy-start | bytes 6291460
  70.1 10.6 %all-to-all-start.2 = ((f32[4,1,128]{2,1,0:T(1,128)}), f32[4,1,128]{2,1,0:T(1,128)S(1)}, u32[]{:S(2)}, u32[]{:S(2)}) async-start(f32[4,1,128]{2,1,0:T(1,128)} %reshape.247), calls=%async_computation.2 | async-start | bytes 4096 | tf_op jit(solution)/shard_map/all_to_all | solution.py:174
  80.7 9.2 %all-to-all-start = ((f32[1,64,512]{2,0,1:T(1,128)}), f32[1,64,512]{2,0,1:T(1,128)S(1)}, u32[]{:S(2)}, u32[]{:S(2)}) async-start(f32[1,64,512]{2,0,1:T(1,128)} %broadcast_in_dim_reshape_reshape.4), calls=%async_computation | async-start | bytes 262144 | tf_op jit(solution)/shard_map/all_to_all | solution.py:175
  84.1 37.5 %all-reduce.6.cloned.1.call-start = ((), (), s32[]{:S(2)}) async-start(), calls=%async_computation.4 | async-start | bytes 131072 | tf_op jit(solution)/shard_map/psum | solution.py:211
Sparse Core Ops, SparseCore 0:
  11.0 39.9 all-reduce.3
  104.7 16.7 all-reduce.5
